TPU v7x, 256 devices: a whole 4x4x8 slice. The times are simulated.
256 devices in a mesh: ep: 64 (over z, x, core), tp: 4 (over y).
Axes of the slice: x: 4, y: 4, z: 8, core: 2. Of those that a mesh axis runs over, the one named last changes fastest.
Arguments:
- conv_input: bfloat16 [65536, 2048], P('ep', 'tp'), may hold values from -6 to 6
- conv_kernel: bfloat16 [31, 2048], P(None, 'tp'), may hold values from -2 to 2
- norm_gain: float32 [2048], P('tp'), may hold values from 0.1 to 1.9
- norm_shift: float32 [2048], P('tp'), may hold values from -3 to 3
- conv_proj: bfloat16 [2048, 2048], P('tp'), may hold values from -0.125 to 0.125
- moe_input: bfloat16 [16384, 2048], P(('ep', 'tp')), may hold values from -6 to 6
- moe_gain: float32 [2048], replicated, may hold values from 0.1 to 1.9
- routes: int32 [16384, 2], P('ep'), may hold values from 0 to 63, all different within a row; in each aligned block of 256 rows (0 to 255, 256 to 511, ...) at most 16 rows name the same one
- route_weights: float32 [16384, 2], P('ep'), may hold values from 0.2 to 1
- gate_proj: bfloat16 [64, 2048, 2048], P('ep', None, 'tp'), may hold values from -0.125 to 0.125
- up_proj: bfloat16 [64, 2048, 2048], P('ep', None, 'tp'), may hold values from -0.125 to 0.125
- down_proj: bfloat16 [64, 2048, 2048], P('ep', 'tp'), may hold values from -0.125 to 0.125
Outputs:
- conv_out: bfloat16 [65536, 2048], P(('ep', 'tp'))
- moe_out: bfloat16 [16384, 2048], P(('ep', 'tp'))
Inputs may be any that keep to these rules, and one draw needn't show every extreme that they name: `routes`: each row names 2 different experts. In each aligned block of 256 rows no expert is named by more than 16 rows, and in some blocks an expert is named by exactly 16 rows.
All inputs are finite; a program needn't handle non-finite values.
Results may differ from a plain program's by a relative error of at most 0.012.
Values may be sent and summed in bfloat16 or wider, within the bound.
No kernel may reach another device: no remote copies, remote signals or barrier semaphores. Data moves between devices by JAX's collectives and lax.ppermute only.
A program may use at most 128 MiB of HBM per device.

v0:
```python
import jax
import jax.numpy as jnp
from jax import lax
from jax.sharding import PartitionSpec as P


def shifted(value, axis, steps):
    count = lax.axis_size(axis)
    leading, last = (max(0, -steps), min(count, count - steps))
    return lax.ppermute(value, axis, [(source, source + steps) for source in range(leading, last)])


def laid_out(tiles, dim):
    lengths = list(tiles.shape[1:])
    lengths[dim] *= tiles.shape[0]
    return jnp.moveaxis(tiles, 0, dim).reshape(lengths)


def from_everyone(array, axis):
    size = lax.axis_size(axis)
    return lax.all_to_all(
        jnp.broadcast_to(array[None], (size, *array.shape)), axis, 0, 0, tiled=True
    )


def collect(array, axis, dim):
    return laid_out(from_everyone(array, axis), dim)


def split_up(array, dim, size):
    before, after = (array.shape[:dim], array.shape[dim + 1 :])
    return jnp.moveaxis(array.reshape(*before, size, -1, *after), dim, 0)


def summed_on_arrival(array, axis, dim):
    tiles = split_up(array, dim, lax.axis_size(axis))
    arrived = lax.all_to_all(tiles, axis, split_axis=0, concat_axis=0, tiled=True)
    return arrived.astype(jnp.float32).sum(axis=0)


def local(
    conv_input,
    conv_kernel,
    norm_gain,
    norm_shift,
    conv_proj,
    moe_input,
    moe_gain,
    routes,
    route_weights,
    gate_proj,
    up_proj,
    down_proj,
):
    tp_count = lax.axis_size("tp")
    ep_count = lax.axis_size("ep")
    local_rows, local_width = conv_input.shape
    reach = conv_kernel.shape[0] - 1
    history = shifted(conv_input[local_rows - reach :], "ep", 1)
    padded = jnp.concatenate([history, conv_input], axis=0)
    taps = conv_kernel.astype(jnp.float32)
    mixed = jnp.zeros((local_rows, local_width), jnp.float32)
    for offset in range(reach + 1):
        mixed = mixed + padded[offset : offset + local_rows].astype(jnp.float32) * taps[offset]
    full_width = local_width * tp_count
    sums, squares = lax.psum((jnp.sum(mixed, axis=1), jnp.sum(mixed * mixed, axis=1)), "tp")
    center = sums / full_width
    spread = jnp.maximum(squares / full_width - center * center, 0.0)
    scaled = (mixed - center[:, None]) * lax.rsqrt(spread[:, None] + 1e-05) * norm_gain + norm_shift
    activated = jax.nn.silu(scaled).astype(jnp.bfloat16)
    rows_taken = activated
    conv_out = lax.psum_scatter(
        jnp.dot(rows_taken, conv_proj, preferred_element_type=jnp.float32).astype(jnp.bfloat16),
        "tp",
        scatter_dimension=0,
        tiled=True,
    )
    moe_float = moe_input.astype(jnp.float32)
    normed = (
        moe_float
        * lax.rsqrt(jnp.mean(moe_float * moe_float, axis=1, keepdims=True) + 1e-06)
        * moe_gain
    ).astype(jnp.bfloat16)
    group = collect(normed, "tp", 0)
    group_rows, top_count = routes.shape
    model_width = group.shape[1]
    capacity = 2 * top_count * group_rows // ep_count
    expert_ids = routes.reshape(-1)
    onehot = (expert_ids[:, None] == jnp.arange(ep_count, dtype=jnp.int32)[None, :]).astype(
        jnp.int32
    )
    ranks = jnp.sum((jnp.cumsum(onehot, axis=0) - onehot) * onehot, axis=1)
    targets = ranks * ep_count + expert_ids
    owners = jnp.arange(group_rows * top_count, dtype=jnp.int32) // top_count
    table = jnp.full((capacity * ep_count,), group_rows, jnp.int32).at[targets].set(owners)
    extended = jnp.concatenate([group, jnp.zeros((1, model_width), jnp.bfloat16)], axis=0)
    outgoing = extended[table].reshape(capacity, ep_count, model_width)
    share = capacity // tp_count
    own_slots = lax.dynamic_slice_in_dim(outgoing, lax.axis_index("tp") * share, share, 0)
    landed = lax.all_to_all(own_slots, "ep", split_axis=1, concat_axis=1, tiled=True)
    arrived = lax.all_gather(landed, "tp", axis=0, tiled=True)
    incoming = arrived.reshape(capacity * ep_count, model_width)
    gated = jax.nn.silu(jnp.dot(incoming, gate_proj[0], preferred_element_type=jnp.float32))
    hidden = (gated * jnp.dot(incoming, up_proj[0], preferred_element_type=jnp.float32)).astype(
        jnp.bfloat16
    )
    weights_flat = route_weights.reshape(-1)
    share = capacity // tp_count
    rows_taken = hidden
    totals = summed_on_arrival(
        jnp.dot(rows_taken, down_proj[0], preferred_element_type=jnp.float32).astype(jnp.bfloat16),
        "tp",
        0,
    )
    returned = lax.all_to_all(
        totals.reshape(share, ep_count, model_width).astype(jnp.bfloat16),
        "ep",
        split_axis=1,
        concat_axis=1,
        tiled=True,
    ).astype(jnp.float32)
    local_slot = ranks - lax.axis_index("tp") * share
    inside = (local_slot >= 0) & (local_slot < share)
    position = jnp.clip(local_slot, 0, share - 1) * ep_count + expert_ids
    picked = jnp.where(inside[:, None], returned.reshape(-1, model_width)[position], 0.0)
    combined = jnp.sum(
        (picked * weights_flat[:, None]).reshape(group_rows, top_count, model_width), axis=1
    )
    moe_out = summed_on_arrival(combined.astype(jnp.bfloat16), "tp", 0).astype(jnp.bfloat16)
    return (conv_out, moe_out)


def solution(mesh):
    placed = (
        P("ep", "tp"),
        P(None, "tp"),
        P("tp"),
        P("tp"),
        P("tp", None),
        P(("ep", "tp"), None),
        P(),
        P("ep", None),
        P("ep", None),
        P("ep", None, "tp"),
        P("ep", None, "tp"),
        P("ep", "tp", None),
    )
    return jax.shard_map(
        local,
        mesh=mesh,
        in_specs=placed,
        out_specs=(P(("ep", "tp"), None), P(("ep", "tp"), None)),
        check_vma=False,
    )
```

profile of v0, /device:TPU:32, one launch (start us, length us, event | category | flops | bytes accessed | tf_op | source)
XLA Modules:
  0.0 319.3 jit_solution(13340980202284212392)
XLA Ops:
  7.2 0.0 copy-start
  7.2 1.3 fusion.43
  8.5 1.1 fusion.45
  9.6 1.1 broadcast_in_dim.15
  10.6 4.5 %all-to-all-start = ((bf16[4,64,2048]{2,1,0:T(8,128)(2,1)}), bf16[4,64,2048]{2,1,0:T(8,128)(2,1)S(1)}, u32[]{:S(2)}, u32[]{:S(2)}) async-start(bf16[4,64,2048]{2,1,0:T(8,128)(2,1)} %broadcast_in_dim.15), calls=%async_computation.1 | async-start | bytes 2097152 | tf_op jit(solution)/shard_map/all_to_all | solution.py:21
  15.1 0.0 copy-done.4
  15.1 0.1 copy.46
  15.3 0.1 eq.29
  15.4 0.1 eq.25
  15.6 1.2 reduce-window.6
  16.8 0.2 slice_reduce_fusion
  17.0 0.1 fusion.48
  17.2 0.1 reshape.158
  17.4 2.4 scatter_custom_fusion
  19.8 10.4 %all-to-all-done = bf16[4,64,2048]{2,1,0:T(8,128)(2,1)S(1)} async-done(((bf16[4,64,2048]{2,1,0:T(8,128)(2,1)}), bf16[4,64,2048]{2,1,0:T(8,128)(2,1)S(1)}, u32[]{:S(2)}, u32[]{:S(2)}) %all-to-all-start) | async-done | bytes 1048608 | tf_op jit(solution)/shard_map/all_to_all | solution.py:21
  30.2 1.0 copy-done.1
  31.2 1.3 concatenate.7
  32.5 6.0 %gather_fusion = bf16[1024,2048]{1,0:T(8,128)(2,1)} fusion(bf16[257,2048]{1,0:T(8,128)(2,1)S(1)} %concatenate.7, s32[1024]{0:T(1024)S(1)} %fusion.50), kind=kCustom, calls=%fused_computation | custom fusion | bytes 8392704 | tf_op jit(solution)/shard_map/gather | solution.py:97
  38.5 1.3 constant_dynamic-slice_fusion
  39.8 0.8 copy.55
  40.6 39.3 %all_to_all.25 = bf16[4,64,2048]{2,0,1:T(4,128)(2,1)S(1)} all-to-all(bf16[4,64,2048]{2,0,1:T(4,128)(2,1)S(1)} %copy.55), channel_id=1, replica_groups=mesh['ep'=64,'tp'=4] {'ep'}, dimensions={1} | all-to-all | bytes 2097152 | tf_op jit(solution)/shard_map/all_to_all | solution.py:100
  79.9 1.6 copy.51
  81.5 0.0 all-gather.2.cloned.1.call-update
  81.5 0.0 reduce-scatter.2.cloned.1.call-start
  81.6 2.2 collective-permute-start
  83.8 5.1 %collective-permute-done = bf16[30,512]{1,0:T(8,128)(2,1)S(1)} collective-permute-done((bf16[30,512]{1,0:T(8,128)(2,1)S(1)}, bf16[30,512]{1,0:T(8,128)(2,1)S(1)}, u32[]{:S(2)}, u32[]{:S(2)}) %collective-permute-start) | collective-permute-done | bytes 30752 | tf_op jit(solution)/shard_map/ppermute | solution.py:10
  88.9 11.2 %fusion.58 = (f32[1024]{0:T(1024)S(1)}, f32[1024]{0:T(1024)S(1)}, f32[1024,512]{1,0:T(8,128)}) fusion(f32[512]{0:T(512)S(1)} %bitcast.117, bf16[1024,512]{1,0:T(8,128)(2,1)S(1)} %copy-done.2, f32[512]{0:T(512)S(1)} %bitcast.116, bf16[30,512]{1,0:T(8,128)(2,1)S(1)} %collective-permute-done, f32[512]{0:T(512)S(1)} %bitcast.115, f32[512]{0:T(512)S(1)} %bitcast.114, ...), kind=kLoop, calls=%fused_computation.121 | loop fusion | flops 96991232 | bytes 3248128 | tf_op jit(solution)/shard_map/reduce_sum | solution.py:66
  100.1 9.8 %all-reduce.1 = (f32[1024]{0:T(1024)S(1)}, f32[1024]{0:T(1024)S(1)}) all-reduce(f32[1024]{0:T(1024)S(1)} %get-tuple-element.3, f32[1024]{0:T(1024)S(1)} %get-tuple-element.2), channel_id=1, replica_groups=mesh['ep'=64,'tp'=4] {'tp'}, use_global_device_ids=true, to_apply=%region_3.0 | all-reduce | flops 2048 | bytes 16384 | tf_op jit(solution)/shard_map/psum | solution.py:66
  109.9 6.3 %convolution_convert_fusion.1 = bf16[1024,2048]{1,0:T(8,128)(2,1)} fusion(bf16[512,2048]{1,0:T(8,128)(2,1)S(1)} %copy-done, f32[1024,512]{1,0:T(8,128)} %get-tuple-element.6, f32[512]{0:T(512)S(1)} %copy-done.6, f32[512]{0:T(512)S(1)} %copy-done.7, f32[1024]{0:T(1024)S(1)} %get-tuple-element.39, f32[1024]{0:T(1024)S(1)} %get-tuple-element.38), kind=kOutput, calls=%fused_computation.34 | convolution fusion | flops 2154299392 | bytes 8400896 | tf_op jit(solution)/shard_map/dot_general | solution.py:73
  116.2 0.0 reduce-scatter.2.cloned.1.call-update
  116.2 12.1 %all-gather.2.cloned.1.call-done = bf16[16,64,2048]{2,1,0:T(8,128)(2,1)} async-done(((bf16[4,64,2048]{2,1,0:T(8,128)(2,1)}), bf16[16,64,2048]{2,1,0:T(8,128)(2,1)}) %all-gather.2.cloned.1.call-update) | async-done | bytes 4194320 | tf_op jit(solution)/shard_map/all_gather | solution.py:101
  128.3 6.6 %fusion.1 = f32[1024,512]{1,0:T(8,128)} fusion(bf16[1024,2048]{1,0:T(8,128)(2,1)} %bitcast.119, bf16[1,2048,512]{2,1,0:T(8,128)(2,1)} %param.22), kind=kOutput, calls=%fused_computation.36 | convolution fusion | flops 2147483648 | bytes 8388608 | tf_op jit(solution)/shard_map/dot_general | solution.py:104
  134.9 10.7 %convolution_convert_fusion = bf16[1024,2048]{1,0:T(8,128)(2,1)} fusion(bf16[1,512,2048]{2,1,0:T(8,128)(2,1)} %param.23, f32[1024,512]{1,0:T(8,128)} %fusion.1, bf16[1024,2048]{1,0:T(8,128)(2,1)} %bitcast.120, bf16[1,2048,512]{2,1,0:T(8,128)(2,1)} %param.21), kind=kOutput, calls=%fused_computation.33 | convolution fusion | flops 4300210176 | bytes 14680064 | tf_op jit(solution)/shard_map/dot_general | solution.py:111
  145.6 79.4 %all_to_all.26 = bf16[4,256,2048]{2,1,0:T(8,128)(2,1)} all-to-all(bf16[4,256,2048]{2,1,0:T(8,128)(2,1)} %bitcast.81), channel_id=1, replica_groups=mesh['ep'=64,'tp'=4] {'tp'}, dimensions={0} | all-to-all | bytes 8388608 | tf_op jit(solution)/shard_map/all_to_all | solution.py:37
  224.9 3.1 reduce_sum.73
  228.0 0.0 copy-start.5
  228.1 1.8 copy.52
  229.8 10.5 %all-to-all-start.3 = ((bf16[4,64,2048]{2,0,1:T(4,128)(2,1)}), bf16[4,64,2048]{2,0,1:T(4,128)(2,1)S(1)}, u32[]{:S(2)}, u32[]{:S(2)}) async-start(bf16[4,64,2048]{2,0,1:T(4,128)(2,1)} %copy.52), calls=%async_computation.4 | async-start | bytes 2097152 | tf_op jit(solution)/shard_map/all_to_all | solution.py:115
  240.3 0.2 and.17
  240.5 0.1 copy.54
  240.7 27.5 %all-to-all-done.3 = bf16[4,64,2048]{2,0,1:T(4,128)(2,1)S(1)} async-done(((bf16[4,64,2048]{2,0,1:T(4,128)(2,1)}), bf16[4,64,2048]{2,0,1:T(4,128)(2,1)S(1)}, u32[]{:S(2)}, u32[]{:S(2)}) %all-to-all-start.3) | async-done | bytes 1048608 | tf_op jit(solution)/shard_map/all_to_all | solution.py:115
  268.2 0.6 copy.53
  268.8 1.7 bitcast_convert_fusion
  270.5 7.0 %gather_fusion.1 = f32[512,2048]{1,0:T(8,128)} fusion(f32[256,2048]{1,0:T(8,128)} %bitcast_convert_fusion, s32[1024]{0:T(1024)S(1)} %pad_clamp_fusion), kind=kCustom, calls=%fused_computation.1 | custom fusion | bytes 8390656 | tf_op jit(solution)/shard_map/gather | solution.py:125
  277.5 5.8 %gather.10 = f32[256,2,2048]{2,1,0:T(2,128)} reshape(f32[512,2048]{1,0:T(8,128)} %gather_fusion.1) | data formatting | bytes 8388608 | tf_op jit(solution)/shard_map/gather | solution.py:125
  283.3 9.9 %multiply_reduce_fusion = bf16[256,2048]{1,0:T(8,128)(2,1)S(1)} fusion(f32[256,2,2048]{2,1,0:T(2,128)} %gather.10, pred[256,2]{1,0:T(8,128)(4,1)S(1)} %and.17, f32[256,2]{1,0:T(8,128)S(1)} %copy.54), kind=kLoop, calls=%fused_computation.32 | loop fusion | flops 2621440 | bytes 5245440 | tf_op jit(solution)/shard_map/reduce_sum | solution.py:126
  293.3 18.2 %all_to_all.27 = bf16[4,64,2048]{2,1,0:T(8,128)(2,1)S(1)} all-to-all(bf16[4,64,2048]{2,1,0:T(8,128)(2,1)S(1)} %bitcast.82), channel_id=1, replica_groups=mesh['ep'=64,'tp'=4] {'tp'}, dimensions={0} | all-to-all | bytes 2097152 | tf_op jit(solution)/shard_map/all_to_all | solution.py:37
  311.5 0.9 reduce_sum.75
  (28 shorter events, 0.2 us)
Async XLA Ops:
  7.2 102.7 %copy-start = (bf16[512,2048]{1,0:T(8,128)(2,1)S(1)}, bf16[512,2048]{1,0:T(8,128)(2,1)}, u32[]{:S(2)}) copy-start(bf16[512,2048]{1,0:T(8,128)(2,1)} %param.16) | copy-start | bytes 6291460
  7.2 7.9 %copy-start.4 = (s32[256,2]{0,1:T(2,128)S(1)}, s32[256,2]{0,1:T(2,128)}, u32[]{:S(2)}) copy-start(s32[256,2]{0,1:T(2,128)} %param.19) | copy-start | bytes 6148
  10.6 19.6 %all-to-all-start = ((bf16[4,64,2048]{2,1,0:T(8,128)(2,1)}), bf16[4,64,2048]{2,1,0:T(8,128)(2,1)S(1)}, u32[]{:S(2)}, u32[]{:S(2)}) async-start(bf16[4,64,2048]{2,1,0:T(8,128)(2,1)} %broadcast_in_dim.15), calls=%async_computation.1 | async-start | bytes 2097152 | tf_op jit(solution)/shard_map/all_to_all | solution.py:21
  15.1 113.2 %all-gather.2.cloned.1.call-start = ((), (), s32[]{:S(2)}) async-start(), calls=%async_computation.7 | async-start | bytes 5242880 | tf_op jit(solution)/shard_map/all_gather | solution.py:101
  30.2 1.0 copy-start.1
  79.9 1.6 copy-start.2
  79.9 3.8 %copy-start.3 = (bf16[31,512]{1,0:T(8,128)(2,1)S(1)}, bf16[31,512]{1,0:T(8,128)(2,1)}, u32[]{:S(2)}) copy-start(bf16[31,512]{1,0:T(8,128)(2,1)} %param.13) | copy-start | bytes 95236
  81.5 28.4 %copy-start.6 = (f32[512]{0:T(512)S(1)}, f32[512]{0:T(512)}, u32[]{:S(2)}) copy-start(f32[512]{0:T(512)} %param.15) | copy-start | bytes 6148
  81.5 28.4 %copy-start.7 = (f32[512]{0:T(512)S(1)}, f32[512]{0:T(512)}, u32[]{:S(2)}) copy-start(f32[512]{0:T(512)} %param.14) | copy-start | bytes 6148
  81.5 230.9 %reduce-scatter.2.cloned.1.call-start = ((), (), s32[]{:S(2)}) async-start(), calls=%async_computation.6 | async-start | bytes 5242880 | tf_op jit(solution)/shard_map/reduce_scatter | solution.py:72
  81.6 7.3 %collective-permute-start = (bf16[30,512]{1,0:T(8,128)(2,1)S(1)}, bf16[30,512]{1,0:T(8,128)(2,1)S(1)}, u32[]{:S(2)}, u32[]{:S(2)}) collective-permute-start(bf16[30,512]{1,0:T(8,128)(2,1)S(1)} %slice.192), channel_id=1, source_target_pairs={{0,4},{4,8},{8,12},{12,16},{16,20},{20,24},{24,28},{28,32},{32,36}... | collective-permute-start | bytes 92168 | tf_op jit(solution)/shard_map/ppermute | solution.py:10
  228.0 12.5 %copy-start.5 = (f32[256,2]{0,1:T(2,128)S(1)}, f32[256,2]{0,1:T(2,128)}, u32[]{:S(2)}) copy-start(f32[256,2]{0,1:T(2,128)} %param.20) | copy-start | bytes 6148
  229.8 38.4 %all-to-all-start.3 = ((bf16[4,64,2048]{2,0,1:T(4,128)(2,1)}), bf16[4,64,2048]{2,0,1:T(4,128)(2,1)S(1)}, u32[]{:S(2)}, u32[]{:S(2)}) async-start(bf16[4,64,2048]{2,0,1:T(4,128)(2,1)} %copy.52), calls=%async_computation.4 | async-start | bytes 2097152 | tf_op jit(solution)/shard_map/all_to_all | solution.py:115
Sparse Core Ops, SparseCore 0:
  81.6 46.6 all-gather.1
  131.4 93.9 reduce-scatter.1
where the time goes:
time: 320 us; the launch traced here: 319 us
  blocking collectives  147 us (46%)
  waiting for transfers between devices  55.2 us (17%)
  local copies, waits for them, and re-layouts  31.9 us (10%)
  other arithmetic  30.6 us (10%)
  matrix products  23.5 us (7%)
  starting transfers between devices  17.1 us (5%)
  between operations  14.3 us (4%)
    all_to_all x2, blocking collectives, summed_on_arrival(): lax.all_to_all(tiles, axis, split_axis=0, concat_axis=0, tiled=True)  97.6 us
    all_to_all x1, blocking collectives, local(): lax.all_to_all(own_slots, 'ep', split_axis=1, concat_axis=1, tiled=True)  39.3 us
    all_to_all x1, waiting for transfers between devices, local(): lax.all_to_all(totals.reshape(share, ep_count, model_width).astype(jnp.bf...  27.5 us
    gather x2, local copies, waits for them, and re-layouts, local(): returned.reshape(-1, model_width)[position]  12.8 us
    all_gather x1, waiting for transfers between devices, local(): arrived = lax.all_gather(landed, 'tp', axis=0, tiled=True)  12.1 us
    reduce_sum x1, other arithmetic, local(): jnp.sum(mixed, axis=1)  11.2 us
    dot_general x1, matrix products, local(): jnp.dot(rows_taken, down_proj[0], preferred_element_type=jnp.float32)  10.7 us
    all_to_all x1, starting transfers between devices, local(): lax.all_to_all(totals.reshape(share, ep_count, model_width).astype(jnp.bf...  10.5 us
  transfers between devices with their start and end apart: 5, of which 4 were waited for; matrix products, arithmetic and copies ran while one was open for 22% of the time, Pallas kernels for 0%

commit v1 on v0

v1 whole, which is shorter than its diff:
```python
import jax
import jax.numpy as jnp
from jax import lax
from jax.sharding import PartitionSpec as P

CHUNKS = 2


def shifted(value, axis, steps):
    count = lax.axis_size(axis)
    leading, last = (max(0, -steps), min(count, count - steps))
    return lax.ppermute(value, axis, [(source, source + steps) for source in range(leading, last)])


def dot(lhs, rhs):
    return jnp.dot(lhs, rhs, preferred_element_type=jnp.float32)


def in_three(value):
    high = lax.reduce_precision(value, 8, 7)
    rest = value - high
    middle = lax.reduce_precision(rest, 8, 7)
    low = rest - middle
    return [term.astype(jnp.bfloat16) for term in (high, middle, low)]


def tied(*values):
    return lax.optimization_barrier(values)


def local(
    conv_input,
    conv_kernel,
    norm_gain,
    norm_shift,
    conv_proj,
    moe_input,
    moe_gain,
    routes,
    route_weights,
    gate_proj,
    up_proj,
    down_proj,
):
    tp_count = lax.axis_size("tp")
    ep_count = lax.axis_size("ep")
    tp_index = lax.axis_index("tp")
    group_rows, top_count = routes.shape
    model_width = moe_input.shape[1]
    capacity = 2 * top_count * group_rows // ep_count
    share = capacity // tp_count
    per = share // CHUNKS

    moe_float = moe_input.astype(jnp.float32)
    normed = (
        moe_float
        * lax.rsqrt(jnp.mean(moe_float * moe_float, axis=1, keepdims=True) + 1e-06)
        * moe_gain
    ).astype(jnp.bfloat16)
    group = lax.all_gather(normed, "tp", axis=0, tiled=True)

    experts = jnp.arange(ep_count, dtype=jnp.int32)
    hits = routes.T[:, None, :] == experts[None, :, None]
    chosen = jnp.any(hits, axis=0)
    weight_of = jnp.sum(jnp.where(hits, route_weights.T[:, None, :], 0.0), axis=0)
    before = (
        lax.broadcasted_iota(jnp.int32, (group_rows, group_rows), 0)
        < lax.broadcasted_iota(jnp.int32, (group_rows, group_rows), 1)
    ).astype(jnp.bfloat16)
    rank = dot(chosen.astype(jnp.bfloat16), before).astype(jnp.int32)
    local_rank = jnp.where(chosen, rank - tp_index * share, -1)

    local_rows, local_width = conv_input.shape
    reach = conv_kernel.shape[0] - 1
    history = shifted(conv_input[local_rows - reach :], "ep", 1)
    padded = jnp.concatenate([history, conv_input], axis=0)
    taps = conv_kernel.astype(jnp.float32)
    mixed = jnp.zeros((local_rows, local_width), jnp.float32)
    for offset in range(reach + 1):
        mixed = mixed + padded[offset : offset + local_rows].astype(jnp.float32) * taps[offset]
    row_sums = (jnp.sum(mixed, axis=1), jnp.sum(mixed * mixed, axis=1))

    group, mixed, *row_sums = tied(group, mixed, *row_sums)

    landed, selected = [], []
    for chunk in range(CHUNKS):
        slots = chunk * per + jnp.arange(per, dtype=jnp.int32)
        select = local_rank[:, None, :] == slots[None, :, None]
        selected.append(select)
        rows = dot(
            select.astype(jnp.bfloat16).reshape(ep_count * per, group_rows), group
        ).astype(jnp.bfloat16)
        if chunk == 0:
            rows, *row_sums = tied(rows, *row_sums)
        landed.append(
            lax.all_to_all(
                rows.reshape(ep_count, per, model_width),
                "ep",
                split_axis=0,
                concat_axis=0,
                tiled=True,
            )
        )

    full_width = local_width * tp_count
    sums, squares = lax.psum(tuple(row_sums), "tp")
    center = sums / full_width
    spread = jnp.maximum(squares / full_width - center * center, 0.0)
    scaled = (mixed - center[:, None]) * lax.rsqrt(spread[:, None] + 1e-05) * norm_gain + norm_shift
    activated = jax.nn.silu(scaled).astype(jnp.bfloat16)
    projected = dot(activated, conv_proj).astype(jnp.bfloat16)
    landed[-1], projected = tied(landed[-1], projected)
    arrived = [lax.all_gather(part, "tp", axis=0, tiled=False) for part in landed]

    totals = []
    for chunk in range(CHUNKS):
        incoming = arrived[chunk].reshape(tp_count * ep_count * per, model_width)
        gated = jax.nn.silu(dot(incoming, gate_proj[0]))
        hidden = (gated * dot(incoming, up_proj[0])).astype(jnp.bfloat16)
        pieces = dot(hidden, down_proj[0]).astype(jnp.bfloat16)
        totals.append(lax.psum_scatter(pieces, "tp", scatter_dimension=0, tiled=True))

    projected, totals[-1] = tied(projected, totals[-1])
    conv_out = lax.psum_scatter(projected, "tp", scatter_dimension=0, tiled=True)

    combined = jnp.zeros((group_rows, model_width), jnp.float32)
    for chunk in range(CHUNKS):
        returned = lax.all_to_all(
            totals[chunk].reshape(ep_count, per, model_width),
            "ep",
            split_axis=0,
            concat_axis=0,
            tiled=True,
        ).reshape(ep_count * per, model_width)
        weights = jnp.where(selected[chunk], weight_of[:, None, :], 0.0)
        for term in in_three(weights.reshape(ep_count * per, group_rows)):
            combined = combined + lax.dot_general(
                term, returned, (((0,), (0,)), ((), ())), preferred_element_type=jnp.float32
            )
    combined, conv_out = tied(combined.astype(jnp.bfloat16), conv_out)
    moe_out = lax.psum_scatter(
        combined, "tp", scatter_dimension=0, tiled=True
    )
    return (conv_out, moe_out)


def solution(mesh):
    placed = (
        P("ep", "tp"),
        P(None, "tp"),
        P("tp"),
        P("tp"),
        P("tp", None),
        P(("ep", "tp"), None),
        P(),
        P("ep", None),
        P("ep", None),
        P("ep", None, "tp"),
        P("ep", None, "tp"),
        P("ep", "tp", None),
    )
    return jax.shard_map(
        local,
        mesh=mesh,
        in_specs=placed,
        out_specs=(P(("ep", "tp"), None), P(("ep", "tp"), None)),
        check_vma=False,
    )
```

time: 320 us -> 302 us (0.944)
  blocking collectives: 147 us -> 36.2 us
  waiting for transfers between devices: 55.2 us -> 142 us
  starting transfers between devices: 17.1 us -> 34 us
  other arithmetic: 30.6 us -> 16.7 us
  matrix products: 23.5 us -> 36.1 us
  local copies, waits for them, and re-layouts: 31.9 us -> 21.7 us
    all_to_all x3 -> x1, blocking collectives: 137 us -> 26.9 us  [local(): lax.all_to_all(rows.reshape(ep_count, per, model_width), 'ep', split_axis...]
    reduce_scatter x1 -> x4, waiting for transfers between devices: 0.01 us -> 89.7 us  [the longest x2 42.2 us: local(): lax.psum_scatter(pieces, 'tp', scatter_dimension=0, tiled=True)]
    all_gather x1 -> x3, waiting for transfers between devices: 12.1 us -> 37.2 us  [the longest x2 25.8 us: local(): lax.all_gather(part, 'tp', axis=0, tiled=False)]
    all_to_all x2 -> x3, waiting for transfers between devices: 37.9 us -> 14.7 us  [the longest x2 14.7 us: local(): lax.all_to_all(totals[chunk].reshape(ep_count, per, model_width), 'ep', s...]
    gather x3 -> x0, local copies, waits for them, and re-layouts: 18.8 us -> none  [the longest x2 12.8 us: local(): returned.reshape(-1, model_width)[position]]
    all_to_all x2 -> x3, starting transfers between devices: 14.9 us -> 31.6 us  [the longest x2 20.9 us: local(): lax.all_to_all(totals[chunk].reshape(ep_count, per, model_width), 'ep', s...]
    reshape x1 -> x6, local copies, waits for them, and re-layouts: 0.14 us -> 14.2 us  [the longest x2 8.32 us: local(): incoming = arrived[chunk].reshape(tp_count * ep_count * per, model_width)]
    dot_general x3 -> x14, matrix products: 23.5 us -> 36.1 us  [the longest x8 30.3 us: dot(): return jnp.dot(lhs, rhs, preferred_element_type=jnp.float32)]
  transfers between devices with their start and end apart: 5 -> 11, of which waited for: 4 -> 8; matrix products, arithmetic and copies ran while one was open for 22% -> 22% of each run, Pallas kernels for 0% -> 0%
where the time goes in v1:
time: 302 us; the launch traced here: 301 us
  waiting for transfers between devices  142 us (47%)
  blocking collectives  36.2 us (12%)
  matrix products  36.1 us (12%)
  starting transfers between devices  34 us (11%)
  local copies, waits for them, and re-layouts  21.7 us (7%)
  other arithmetic  16.7 us (6%)
  between operations  14.4 us (5%)
    reduce_scatter x2, waiting for transfers between devices, local(): lax.psum_scatter(pieces, 'tp', scatter_dimension=0, tiled=True)  42.2 us
    dot_general x8, matrix products, dot(): return jnp.dot(lhs, rhs, preferred_element_type=jnp.float32)  30.3 us
    reduce_scatter x1, waiting for transfers between devices, local(): moe_out = lax.psum_scatter(combined, 'tp', scatter_dimension=0, tiled=True)  29.2 us
    all_to_all x1, blocking collectives, local(): lax.all_to_all(rows.reshape(ep_count, per, model_width), 'ep', split_axis...  26.9 us
    all_gather x2, waiting for transfers between devices, local(): lax.all_gather(part, 'tp', axis=0, tiled=False)  25.8 us
    all_to_all x2, starting transfers between devices, local(): lax.all_to_all(totals[chunk].reshape(ep_count, per, model_width), 'ep', s...  20.9 us
    reduce_scatter x1, waiting for transfers between devices, local(): lax.psum_scatter(projected, 'tp', scatter_dimension=0, tiled=True)  18.4 us
    all_to_all x2, waiting for transfers between devices, local(): lax.all_to_all(totals[chunk].reshape(ep_count, per, model_width), 'ep', s...  14.7 us
  transfers between devices with their start and end apart: 11, of which 8 were waited for; matrix products, arithmetic and copies ran while one was open for 22% of the time, Pallas kernels for 0%

profile of v1, /device:TPU:32, one launch (start us, length us, event | category | flops | bytes accessed | tf_op | source)
XLA Modules:
  0.0 300.9 jit_solution(8955935681420171659)
XLA Ops:
  7.2 0.9 slice.186
  8.2 1.9 collective-permute-start
  10.1 1.1 fusion.68
  11.2 1.8 fusion.70
  13.1 1.6 fusion.119
  14.6 1.8 fusion.118
  16.5 0.7 fusion.81
  17.2 0.2 fusion.29
  17.4 0.7 eq.79
  18.1 0.7 eq.73
  18.8 0.1 eq.71
  18.9 13.1 %multiply_reduce_fusion = (f32[1024]{0:T(1024)S(1)}, f32[1024]{0:T(1024)S(1)}, f32[1024,512]{1,0:T(8,128)}) fusion(f32[512]{0:T(512)} %bitcast.105, bf16[1024,512]{1,0:T(8,128)(2,1)S(1)} %copy-done.4, f32[512]{0:T(512)} %bitcast.104, bf16[30,512]{1,0:T(8,128)(2,1)S(1)} %collective-permute-done, f32[512]{0:T(512)} %bitcast.103, f32[512]{0:T(512)} %bitcast.102, ...), kind=kLoop, calls=%fused_computation.57 | loop fusion | flops 96991232 | bytes 3248128 | tf_op jit(solution)/shard_map/reduce_sum | solution.py:81
  32.0 11.4 %all-gather.6.cloned.1.call-done = bf16[256,2048]{1,0:T(8,128)(2,1)} async-done(((bf16[64,2048]{1,0:T(8,128)(2,1)}), bf16[256,2048]{1,0:T(8,128)(2,1)}) %all-gather.6.cloned.1.call-update) | async-done | bytes 1048592 | tf_op jit(solution)/shard_map/all_gather | solution.py:60
  43.4 2.5 convolution_convert_fusion.3
  45.9 2.2 reshape.100
  48.1 10.7 %all-to-all-start.2 = ((bf16[64,2,2048]{2,1,0:T(2,128)(2,1)}), bf16[64,2,2048]{2,1,0:T(2,128)(2,1)}, u32[]{:S(2)}, u32[]{:S(2)}) async-start(bf16[64,2,2048]{2,1,0:T(2,128)(2,1)} %reshape.100), calls=%async_computation.3 | async-start | bytes 1048576 | tf_op jit(solution)/shard_map/all_to_all | solution.py:96
  58.9 1.1 convolution_convert_fusion.4
  60.0 9.3 %all-reduce = (f32[1024]{0:T(1024)S(1)}, f32[1024]{0:T(1024)S(1)}) all-reduce(f32[1024]{0:T(1024)S(1)} %get-tuple-element.21, f32[1024]{0:T(1024)S(1)} %get-tuple-element.20), channel_id=1, replica_groups=mesh['ep'=64,'tp'=4] {'tp'}, use_global_device_ids=true, to_apply=%region_7.8 | all-reduce | flops 2048 | bytes 16384 | tf_op jit(solution)/shard_map/psum | solution.py:106
  69.4 6.3 %convolution_convert_fusion = bf16[1024,2048]{1,0:T(8,128)(2,1)} fusion(bf16[512,2048]{1,0:T(8,128)(2,1)S(1)} %copy-done, f32[1024,512]{1,0:T(8,128)} %get-tuple-element.19, f32[512]{0:T(512)S(1)} %copy-done.10, f32[512]{0:T(512)S(1)} %copy-done.11, f32[1024]{0:T(1024)S(1)} %get-tuple-element.65, f32[1024]{0:T(1024)S(1)} %get-tuple-element.64), kind=kOutput, calls=%fused_computation.29 | convolution fusion | flops 2154299392 | bytes 8400896 | tf_op jit(solution)/shard_map/dot_general | solution.py:16
  75.9 0.3 reshape.97
  76.2 26.9 %all_to_all.20 = bf16[64,2,2048]{2,1,0:T(2,128)(2,1)} all-to-all(bf16[64,2,2048]{2,1,0:T(2,128)(2,1)S(1)} %reshape.97), channel_id=1, replica_groups=mesh['ep'=64,'tp'=4] {'ep'}, dimensions={0} | all-to-all | bytes 1048576 | tf_op jit(solution)/shard_map/all_to_all | solution.py:96
  103.1 5.1 %all-gather.10.cloned.1.call-done = bf16[256,2,2048]{2,1,0:T(2,128)(2,1)} async-done(((bf16[64,2,2048]{2,1,0:T(2,128)(2,1)}), bf16[256,2,2048]{2,1,0:T(2,128)(2,1)}) %all-gather.10.cloned.1.call-update) | async-done | bytes 2097168 | tf_op jit(solution)/shard_map/all_gather | solution.py:113
  108.3 4.2 %reshape.101 = bf16[512,2048]{1,0:T(8,128)(2,1)} reshape(bf16[256,2,2048]{2,1,0:T(2,128)(2,1)} %all-gather.10.cloned.1.call-done) | data formatting | bytes 4194304 | tf_op jit(solution)/shard_map/reshape | solution.py:117
  112.4 3.5 %fusion.12 = f32[512,512]{1,0:T(8,128)S(1)} fusion(bf16[512,2048]{1,0:T(8,128)(2,1)} %reshape.101, bf16[1,2048,512]{2,1,0:T(8,128)(2,1)} %param.21), kind=kOutput, calls=%fused_computation.52 | convolution fusion | flops 1073741824 | bytes 5242880 | tf_op jit(solution)/shard_map/dot_general | solution.py:16
  115.9 6.6 %convolution_convert_fusion.1 = bf16[512,2048]{1,0:T(8,128)(2,1)} fusion(bf16[1,512,2048]{2,1,0:T(8,128)(2,1)} %param.23, bf16[512,2048]{1,0:T(8,128)(2,1)} %reshape.101, bf16[1,2048,512]{2,1,0:T(8,128)(2,1)} %param.22, f32[512,512]{1,0:T(8,128)S(1)} %fusion.12), kind=kOutput, calls=%fused_computation.30 | convolution fusion | flops 2150105088 | bytes 9437184 | tf_op jit(solution)/shard_map/dot_general | solution.py:16
  122.6 0.2 reduce-scatter.5.cloned.1.call-start
  122.8 20.7 %all-gather.8.cloned.1.call-done = bf16[256,2,2048]{2,1,0:T(2,128)(2,1)} async-done(((bf16[64,2,2048]{2,1,0:T(2,128)(2,1)}), bf16[256,2,2048]{2,1,0:T(2,128)(2,1)}) %all-gather.8.cloned.1.call-update) | async-done | bytes 2097168 | tf_op jit(solution)/shard_map/all_gather | solution.py:113
  143.5 4.2 %reshape.98 = bf16[512,2048]{1,0:T(8,128)(2,1)} reshape(bf16[256,2,2048]{2,1,0:T(2,128)(2,1)} %all-gather.8.cloned.1.call-done) | data formatting | bytes 4194304 | tf_op jit(solution)/shard_map/reshape | solution.py:117
  147.7 3.5 %fusion.14 = f32[512,512]{1,0:T(8,128)S(1)} fusion(bf16[512,2048]{1,0:T(8,128)(2,1)} %reshape.98, bf16[1,2048,512]{2,1,0:T(8,128)(2,1)} %param.21), kind=kOutput, calls=%fused_computation.54 | convolution fusion | flops 1073741824 | bytes 5242880 | tf_op jit(solution)/shard_map/dot_general | solution.py:16
  151.1 6.7 %convolution_convert_fusion.2 = bf16[512,2048]{1,0:T(8,128)(2,1)} fusion(bf16[1,512,2048]{2,1,0:T(8,128)(2,1)} %param.23, bf16[512,2048]{1,0:T(8,128)(2,1)} %reshape.98, bf16[1,2048,512]{2,1,0:T(8,128)(2,1)} %param.22, f32[512,512]{1,0:T(8,128)S(1)} %fusion.14), kind=kOutput, calls=%fused_computation.31 | convolution fusion | flops 2150105088 | bytes 9437184 | tf_op jit(solution)/shard_map/dot_general | solution.py:16
  157.9 20.4 %reduce-scatter.7.cloned.1.call-done = bf16[128,2048]{1,0:T(8,128)(2,1)} async-done(((bf16[512,2048]{1,0:T(8,128)(2,1)}), bf16[128,2048]{1,0:T(8,128)(2,1)}) %reduce-scatter.7.cloned.1.call-update) | async-done | bytes 524304 | tf_op jit(solution)/shard_map/reduce_scatter | solution.py:121
  178.3 1.0 copy-done.5
  179.3 1.1 reshape.102
  180.4 10.5 %all-to-all-start.3 = ((bf16[64,2,2048]{2,1,0:T(2,128)(2,1)}), bf16[64,2,2048]{2,1,0:T(2,128)(2,1)S(1)}, u32[]{:S(2)}, u32[]{:S(2)}) async-start(bf16[64,2,2048]{2,1,0:T(2,128)(2,1)} %reshape.102), calls=%async_computation.5 | async-start | bytes 1048576 | tf_op jit(solution)/shard_map/all_to_all | solution.py:128
  190.9 21.8 %reduce-scatter.5.cloned.1.call-done = bf16[128,2048]{1,0:T(8,128)(2,1)} async-done(((bf16[512,2048]{1,0:T(8,128)(2,1)}), bf16[128,2048]{1,0:T(8,128)(2,1)}) %reduce-scatter.5.cloned.1.call-update) | async-done | bytes 524304 | tf_op jit(solution)/shard_map/reduce_scatter | solution.py:121
  212.7 2.2 reshape.99
  214.9 10.4 %all-to-all-start.1 = ((bf16[64,2,2048]{2,1,0:T(2,128)(2,1)}), bf16[64,2,2048]{2,1,0:T(2,128)(2,1)S(1)}, u32[]{:S(2)}, u32[]{:S(2)}) async-start(bf16[64,2,2048]{2,1,0:T(2,128)(2,1)} %reshape.99), calls=%async_computation.2 | async-start | bytes 1048576 | tf_op jit(solution)/shard_map/all_to_all | solution.py:128
  225.3 0.0 reduce-scatter.11.cloned.1.call-start
  225.4 1.9 convolution_bitcast_fusion.2
  227.3 14.7 %all-to-all-done.1 = bf16[64,2,2048]{2,1,0:T(2,128)(2,1)S(1)} async-done(((bf16[64,2,2048]{2,1,0:T(2,128)(2,1)}), bf16[64,2,2048]{2,1,0:T(2,128)(2,1)S(1)}, u32[]{:S(2)}, u32[]{:S(2)}) %all-to-all-start.1) | async-done | bytes 524320 | tf_op jit(solution)/shard_map/all_to_all | solution.py:128
  242.0 0.5 convolution_bitcast_fusion.4
  242.5 0.5 convolution_bitcast_fusion.1
  243.0 0.5 convolution_bitcast_fusion.3
  243.5 0.5 convolution_bitcast_fusion
  244.0 0.6 copy-done.1
  244.6 1.9 fusion.5
  246.5 18.4 %reduce-scatter.9.cloned.1.call-done = bf16[256,2048]{1,0:T(8,128)(2,1)} async-done(((bf16[1024,2048]{1,0:T(8,128)(2,1)}), bf16[256,2048]{1,0:T(8,128)(2,1)}) %reduce-scatter.9.cloned.1.call-update) | async-done | bytes 1048592 | tf_op jit(solution)/shard_map/reduce_scatter | solution.py:124
  264.9 29.2 %reduce-scatter.11.cloned.1.call-done = bf16[64,2048]{1,0:T(8,128)(2,1)} async-done(((bf16[256,2048]{1,0:T(8,128)(2,1)}), bf16[64,2048]{1,0:T(8,128)(2,1)}) %reduce-scatter.11.cloned.1.call-update) | async-done | bytes 262160 | tf_op jit(solution)/shard_map/reduce_scatter | solution.py:141
  (44 shorter events, 0.5 us)
Async XLA Ops:
  7.2 62.2 %copy-start = (bf16[512,2048]{1,0:T(8,128)(2,1)S(1)}, bf16[512,2048]{1,0:T(8,128)(2,1)}, u32[]{:S(2)}) copy-start(bf16[512,2048]{1,0:T(8,128)(2,1)} %param.16) | copy-start | bytes 6291460
  7.2 11.7 %copy-start.4 = (bf16[1024,512]{1,0:T(8,128)(2,1)S(1)}, bf16[1024,512]{1,0:T(8,128)(2,1)}, u32[]{:S(2)}) copy-start(bf16[1024,512]{1,0:T(8,128)(2,1)} %param.12) | copy-start | bytes 3145732
  7.2 36.3 %all-gather.6.cloned.1.call-start = ((), (), s32[]{:S(2)}) async-start(), calls=%async_computation.8 | async-start | bytes 1310720 | tf_op jit(solution)/shard_map/all_gather | solution.py:60
  8.2 10.7 %collective-permute-start = (bf16[30,512]{1,0:T(8,128)(2,1)S(1)}, bf16[30,512]{1,0:T(8,128)(2,1)S(1)}, u32[]{:S(2)}, u32[]{:S(2)}) collective-permute-start(bf16[30,512]{1,0:T(8,128)(2,1)S(1)} %slice.186), channel_id=1, source_target_pairs={{0,4},{4,8},{8,12},{12,16},{16,20},{20,24},{24,28},{28,32},{32,36}... | collective-permute-start | bytes 92168 | tf_op jit(solution)/shard_map/ppermute | solution.py:12
  18.9 24.6 %copy-start.8 = (s32[128]{0:T(128)S(1)}, s32[128]{0:T(128)}, u32[]{:S(2)}) copy-start(s32[128]{0:T(128)} %eq.79) | copy-start | bytes 1540
  32.0 26.8 %copy-start.7 = (s32[128]{0:T(128)S(1)}, s32[128]{0:T(128)}, u32[]{:S(2)}) copy-start(s32[128]{0:T(128)} %eq.73) | copy-start | bytes 1540
  43.4 15.4 %copy-start.2 = (bf16[256,2048]{1,0:T(8,128)(2,1)S(1)}, bf16[256,2048]{1,0:T(8,128)(2,1)}, u32[]{:S(2)}) copy-start(bf16[256,2048]{1,0:T(8,128)(2,1)} %all-gather.6.cloned.1.call-done) | copy-start | bytes 3145732
  45.9 23.5 %copy-start.10 = (f32[512]{0:T(512)S(1)}, f32[512]{0:T(512)}, u32[]{:S(2)}) copy-start(f32[512]{0:T(512)} %param.15) | copy-start | bytes 6148
  45.9 23.5 %copy-start.11 = (f32[512]{0:T(512)S(1)}, f32[512]{0:T(512)}, u32[]{:S(2)}) copy-start(f32[512]{0:T(512)} %param.14) | copy-start | bytes 6148
  48.1 27.6 %all-to-all-start.2 = ((bf16[64,2,2048]{2,1,0:T(2,128)(2,1)}), bf16[64,2,2048]{2,1,0:T(2,128)(2,1)}, u32[]{:S(2)}, u32[]{:S(2)}) async-start(bf16[64,2,2048]{2,1,0:T(2,128)(2,1)} %reshape.100), calls=%async_computation.3 | async-start | bytes 1048576 | tf_op jit(solution)/shard_map/all_to_all | solution.py:96
  58.8 49.5 %all-gather.10.cloned.1.call-start = ((), (), s32[]{:S(2)}) async-start(), calls=%async_computation.14 | async-start | bytes 2621440 | tf_op jit(solution)/shard_map/all_gather | solution.py:113
  69.4 6.4 %copy-start.3 = (bf16[128,2048]{1,0:T(8,128)(2,1)S(1)}, bf16[128,2048]{1,0:T(8,128)(2,1)}, u32[]{:S(2)}) copy-start(bf16[128,2048]{1,0:T(8,128)(2,1)} %convolution_convert_fusion.4) | copy-start | bytes 1572868
  75.8 67.7 %all-gather.8.cloned.1.call-start = ((), (), s32[]{:S(2)}) async-start(), calls=%async_computation.13 | async-start | bytes 2621440 | tf_op jit(solution)/shard_map/all_gather | solution.py:113
  103.1 75.2 %reduce-scatter.7.cloned.1.call-start = ((), (), s32[]{:S(2)}) async-start(), calls=%async_computation.10 | async-start | bytes 2621440 | tf_op jit(solution)/shard_map/reduce_scatter | solution.py:121
  122.6 90.1 %reduce-scatter.5.cloned.1.call-start = ((), (), s32[]{:S(2)}) async-start(), calls=%async_computation.9 | async-start | bytes 2621440 | tf_op jit(solution)/shard_map/reduce_scatter | solution.py:121
  157.8 107.0 %reduce-scatter.9.cloned.1.call-start = ((), (), s32[]{:S(2)}) async-start(), calls=%async_computation.11 | async-start | bytes 5242880 | tf_op jit(solution)/shard_map/reduce_scatter | solution.py:124
  178.3 1.0 copy-start.5
  179.3 46.1 %copy-start.6 = (s32[256,2]{0,1:T(2,128)S(1)}, s32[256,2]{0,1:T(2,128)}, u32[]{:S(2)}) copy-start(s32[256,2]{0,1:T(2,128)} %param.19) | copy-start | bytes 6148
  179.3 46.1 %copy-start.9 = (f32[256,2]{0,1:T(2,128)S(1)}, f32[256,2]{0,1:T(2,128)}, u32[]{:S(2)}) copy-start(f32[256,2]{0,1:T(2,128)} %param.20) | copy-start | bytes 6148
  180.4 34.4 %all-to-all-start.3 = ((bf16[64,2,2048]{2,1,0:T(2,128)(2,1)}), bf16[64,2,2048]{2,1,0:T(2,128)(2,1)S(1)}, u32[]{:S(2)}, u32[]{:S(2)}) async-start(bf16[64,2,2048]{2,1,0:T(2,128)(2,1)} %reshape.102), calls=%async_computation.5 | async-start | bytes 1048576 | tf_op jit(solution)/shard_map/all_to_all | solution.py:128
  214.9 27.1 %all-to-all-start.1 = ((bf16[64,2,2048]{2,1,0:T(2,128)(2,1)}), bf16[64,2,2048]{2,1,0:T(2,128)(2,1)S(1)}, u32[]{:S(2)}, u32[]{:S(2)}) async-start(bf16[64,2,2048]{2,1,0:T(2,128)(2,1)} %reshape.99), calls=%async_computation.2 | async-start | bytes 1048576 | tf_op jit(solution)/shard_map/all_to_all | solution.py:128
  225.3 68.7 %reduce-scatter.11.cloned.1.call-start = ((), (), s32[]{:S(2)}) async-start(), calls=%async_computation.12 | async-start | bytes 1310720 | tf_op jit(solution)/shard_map/reduce_scatter | solution.py:141
  243.0 1.6 copy-start.1
Sparse Core Ops, SparseCore 0:
  13.2 30.2 all-gather.5
  75.9 32.3 all-gather.9
  110.1 33.3 all-gather.7
  145.9 32.3 reduce-scatter.6
  180.6 31.9 reduce-scatter.4
  215.7 49.1 reduce-scatter.8
  268.0 26.0 reduce-scatter.10
